TPU v7x, 32 devices: a whole 2x2x4 slice. The times are simulated.
32 devices in a mesh: ep: 4 (over y, x), tp: 8 (over z, core).
Axes of the slice: x: 2, y: 2, z: 4, core: 2. Of those that a mesh axis runs over, the one named last changes fastest.
Arguments:
- tokens: bfloat16 [128, 4096], P('ep'), may hold values from -6 to 6
- norm_gain: float32 [4096], replicated, may hold values from 0.1 to 1.9
- group_ids: int32 [128, 1], P('ep'), may hold values from 0 to 1; in each aligned block of 32 rows (0 to 31, 32 to 63, ...) at most 32 rows name the same one
- local_ids: int32 [128, 4], P('ep'), may hold values from 0 to 7, all different within a row
- group_gate: float32 [128], P('ep'), may hold values from 0.3 to 1
- expert_gate: float32 [128, 4], P('ep'), may hold values from 0.1 to 1
- lengths: int32 [32], P('ep'), may hold values from 1 to 4, 64 in all
- w_gate: bfloat16 [16, 1024, 4096], P('ep', 'tp'), may hold values from -0.09375 to 0.09375
- w_up: bfloat16 [16, 1024, 4096], P('ep', 'tp'), may hold values from -0.09375 to 0.09375
- w_down: bfloat16 [16, 1024, 4096], P('ep', None, 'tp'), may hold values from -0.1875 to 0.1875
Outputs:
- mixed: bfloat16 [128, 4096], P('ep', 'tp')
Inputs may be any that keep to these rules, and one draw needn't show every extreme that they name: `group_ids`: among the 32 rows of one index of ep no group is named by more than 32 rows, and some index reaches 32. `local_ids`: each row names 4 different experts of its group. `lengths`: the first that many of a sequence's 4 positions are live.
All inputs are finite; a program needn't handle non-finite values. No bound on the sum of `lengths` on one device may be relied on, other than what follows from the above.
Results may differ from a plain program's by a relative error of at most 0.0065.
Values may be sent and summed in bfloat16 or wider, within the bound.
A program may use at most 64 MiB of HBM per device.

v0:
```python
import jax
import jax.numpy as jnp
from jax import lax
from jax.sharding import PartitionSpec as P

EXP_PER_GROUP = 8
STEP_TOK = 4


def norm_rows(tokens, norm_gain):
    values = tokens.astype(jnp.float32)
    scale = lax.rsqrt(jnp.mean(values * values, axis=1, keepdims=True) + 1e-06)
    return (values * scale * norm_gain).astype(jnp.bfloat16)


def live_mask(lengths, tok_rows):
    places = jnp.arange(tok_rows, dtype=jnp.int32)
    within = places % STEP_TOK
    owner = places // STEP_TOK
    seq_ids = jnp.arange(lengths.shape[0], dtype=jnp.int32)
    hits = (owner[:, None] == seq_ids[None, :]) & (within[:, None] < lengths[None, :])
    return jnp.any(hits, axis=1).astype(jnp.float32)


def expert_hidden(rows, w_gate, w_up):
    gate_part = jnp.einsum("rd,efd->ref", rows, w_gate, preferred_element_type=jnp.float32)
    up_part = jnp.einsum("rd,efd->ref", rows, w_up, preferred_element_type=jnp.float32)
    return (jax.nn.silu(gate_part) * up_part).astype(jnp.bfloat16)


def local(
    tokens, norm_gain, group_ids, local_ids, group_gate, expert_gate, lengths, w_gate, w_up, w_down
):
    highest = lax.Precision.HIGHEST
    tok_rows = tokens.shape[0]
    exp_dev = w_gate.shape[0]
    width_part = w_down.shape[2]
    ep_size = lax.axis_size("ep")
    groups = exp_dev * ep_size // EXP_PER_GROUP
    normed = norm_rows(tokens, norm_gain)
    live = live_mask(lengths, tok_rows)
    local_cols = jnp.arange(EXP_PER_GROUP, dtype=jnp.int32)
    picks = (local_ids[:, :, None] == local_cols[None, None, :]).astype(jnp.float32)
    weights = expert_gate * (group_gate * live)[:, None]
    dense = jnp.sum(picks * weights[:, :, None], axis=1)
    group_cols = jnp.arange(groups, dtype=jnp.int32)
    member_int = (group_ids == group_cols[None, :]).astype(jnp.int32)
    member = member_int.astype(jnp.float32)
    capacity = 2 * tok_rows // groups
    counts = jnp.cumsum(member_int, axis=0)
    rank = jnp.sum((counts - 1) * member_int, axis=1)
    slot_ids = jnp.arange(capacity, dtype=jnp.int32)
    select = member.T[:, None, :] * (rank[None, None, :] == slot_ids[None, :, None]).astype(
        jnp.float32
    )
    rows_by_group = jnp.einsum(
        "gct,td->gcd", select.astype(jnp.bfloat16), normed, preferred_element_type=jnp.float32
    ).astype(jnp.bfloat16)
    gates_by_group = jnp.einsum("gct,tl->gcl", select, dense, precision=highest)
    share = EXP_PER_GROUP // exp_dev
    send_rows = jnp.repeat(rows_by_group, share, axis=0)
    send_gates = gates_by_group.reshape(groups, capacity, share, exp_dev).transpose(0, 2, 1, 3)
    send_gates = send_gates.reshape(ep_size, capacity, exp_dev)
    recv_rows = lax.all_to_all(send_rows, "ep", split_axis=0, concat_axis=0, tiled=True)
    recv_gates = lax.all_to_all(send_gates, "ep", split_axis=0, concat_axis=0, tiled=True)
    slot_rows = recv_rows.reshape(ep_size * capacity, recv_rows.shape[2])
    slot_gates = recv_gates.reshape(ep_size * capacity, exp_dev)
    hidden = expert_hidden(slot_rows, w_gate, w_up)
    total = jnp.einsum(
        "ref,efd->red",
        lax.all_gather(hidden, "tp", axis=2, tiled=True),
        w_down,
        preferred_element_type=jnp.float32,
    )
    results = jnp.einsum("re,red->rd", slot_gates, total, precision=highest)
    results = results.reshape(ep_size, capacity, width_part)
    back = lax.all_to_all(results, "ep", split_axis=0, concat_axis=0, tiled=True)
    grouped = jnp.sum(back.reshape(groups, share, capacity, width_part), axis=1)
    mixed = jnp.einsum("gct,gcd->td", select, grouped, precision=highest)
    return mixed.astype(jnp.bfloat16)


def solution(mesh):
    in_specs = (
        P("ep", None),
        P(),
        P("ep", None),
        P("ep", None),
        P("ep"),
        P("ep", None),
        P("ep"),
        P("ep", "tp", None),
        P("ep", "tp", None),
        P("ep", None, "tp"),
    )
    out_specs = P("ep", "tp")
    return jax.shard_map(local, mesh=mesh, in_specs=in_specs, out_specs=out_specs, check_vma=False)
```

profile of v0, /device:TPU:0, one launch (start us, length us, event | category | flops | bytes accessed | tf_op | source)
XLA Modules:
  0.0 81.1 jit_solution(2347612556403566781)
XLA Ops:
  6.5 0.7 fusion.25
  7.2 0.7 fusion.17
  7.9 1.1 %fusion.4 = f32[32]{0:T(128)S(1)} fusion(bf16[32,4096]{1,0:T(8,128)(2,1)} %param.10), kind=kLoop, calls=%fused_computation.10 | loop fusion | flops 393184 | bytes 262272 | tf_op jit(solution)/shard_map/reduce_sum | solution.py:12
  9.0 0.1 reduce_window_sum.11
  9.1 1.0 %select_reduce_fusion.1 = s32[32]{0:T(128)S(1)} fusion(s32[32,2]{1,0:T(8,128)S(1)} %reduce_window_sum.11, s32[32]{0:T(128)} %bitcast.46), kind=kLoop, calls=%fused_computation.27 | loop fusion | flops 224 | bytes 512 | tf_op jit(solution)/shard_map/reduce_sum | solution.py:51
  10.1 0.1 fusion.21
  10.2 1.6 %convolution_convert_fusion = bf16[2,32,4096]{2,1,0:T(8,128)(2,1)S(1)} fusion(bf16[32,4096]{1,0:T(8,128)(2,1)} %param.10, f32[4096]{0:T(1024)} %param.11, f32[32]{0:T(128)S(1)} %add_rsqrt_fusion, f32[32,32]{0,1:T(8,128)S(1)} %fusion.21, f32[2,32]{1,0:T(2,128)S(1)} %fusion.25), kind=kOutput, calls=%fused_computation | convolution fusion | flops 17567744 | bytes 807296 | tf_op jit(solution)/shard_map/gct,td->gcd/dot_general | solution.py:56
  11.7 0.1 broadcast_in_dim.2
  11.8 0.0 copy-start.4
  11.8 19.4 %all_to_all.15 = bf16[4,32,4096]{2,1,0:T(8,128)(2,1)S(1)} all-to-all(bf16[4,32,4096]{2,1,0:T(8,128)(2,1)S(1)} %bitcast.37), channel_id=1, replica_groups=mesh['ep'=4,'tp'=8] {'ep'}, dimensions={0} | all-to-all | bytes 2097152 | tf_op jit(solution)/shard_map/all_to_all | solution.py:64
  31.3 1.5 %fusion.27 = f32[128,4,128]{2,0,1:T(8,128)S(1)} fusion(bf16[128,4096,1]{1,0,2:T(8,128)(2,1)S(1)} %bitcast.38, bf16[4,128,4096]{2,1,0:T(8,128)(2,1)S(1)} %copy-done), kind=kOutput, calls=%fused_computation.51 | convolution fusion | flops 536870912 | bytes 5505024 | tf_op jit(solution)/shard_map/rd,efd->ref/dot_general | solution.py:26
  32.8 0.0 copy-start.3
  32.8 0.0 copy-start.5
  32.8 0.0 copy-start.1
  32.8 0.0 copy-start.2
  32.8 2.2 %fusion = bf16[128,4,128]{2,0,1:T(8,128)(2,1)} fusion(bf16[128,4096,1]{1,0,2:T(8,128)(2,1)S(1)} %bitcast.39, bf16[4,128,4096]{2,1,0:T(8,128)(2,1)S(1)} %copy-done.4, f32[128,4,128]{2,0,1:T(8,128)S(1)} %fusion.27), kind=kOutput, calls=%fused_computation.3 | convolution fusion | flops 537264128 | bytes 5636096 | tf_op jit(solution)/shard_map/rd,efd->ref/dot_general | solution.py:27
  35.0 0.0 all-gather.2.cloned.1.call-update
  35.1 0.1 fusion.24
  35.2 0.2 fusion.12
  35.4 0.1 pad_maximum_fusion
  35.5 0.1 reshape.102
  35.6 0.1 reshape.115
  35.7 7.0 %all_to_all.16 = f32[4,1,128]{2,1,0:T(1,128)S(1)} all-to-all(f32[4,1,128]{2,1,0:T(1,128)S(1)} %reshape.115), channel_id=1, replica_groups=mesh['ep'=4,'tp'=8] {'ep'}, dimensions={0} | all-to-all | bytes 4096 | tf_op jit(solution)/shard_map/all_to_all | solution.py:65
  42.7 0.5 broadcast.120
  43.2 0.7 reduce
  43.9 0.1 reshape.116
  44.0 0.1 copy.43
  44.1 14.7 %all-gather.2.cloned.1.call-done = bf16[128,4,1024]{2,0,1:T(8,128)(2,1)} async-done(((bf16[128,4,128]{2,0,1:T(8,128)(2,1)}), bf16[128,4,1024]{2,0,1:T(8,128)(2,1)}) %all-gather.2.cloned.1.call-update) | async-done | bytes 1048592 | tf_op jit(solution)/shard_map/all_gather | solution.py:71
  58.8 3.2 %convolution_bitcast_fusion = f32[128,4,512]{2,0,1:T(8,128)S(1)} fusion(bf16[128,4,1024]{2,0,1:T(8,128)(2,1)} %all-gather.2.cloned.1.call-done, bf16[4,1024,512]{2,1,0:T(8,128)(2,1)} %param.19), kind=kOutput, calls=%fused_computation.1 | convolution fusion | flops 536870912 | bytes 6291456 | tf_op jit(solution)/shard_map/ref,efd->red/dot_general | solution.py:69
  62.0 2.4 %fusion.2 = f32[128,1,512]{2,1,0:T(1,128)S(1)} fusion(f32[128,4,1]{1,2,0:T(1,128)S(1)} %bitcast.41, f32[128,4,512]{2,0,1:T(8,128)S(1)} %convolution_bitcast_fusion), kind=kOutput, calls=%fused_computation.6 | convolution fusion | flops 3145728 | bytes 1312768 | tf_op jit(solution)/shard_map/re,red->rd/dot_general | solution.py:75
  64.5 8.8 %all_to_all.17 = f32[4,32,512]{2,1,0:T(8,128)S(1)} all-to-all(f32[4,32,512]{2,1,0:T(8,128)S(1)} %bitcast.40), channel_id=1, replica_groups=mesh['ep'=4,'tp'=8] {'ep'}, dimensions={0} | all-to-all | bytes 524288 | tf_op jit(solution)/shard_map/all_to_all | solution.py:77
  73.3 0.9 %fusion.1 = bf16[32,512]{1,0:T(8,128)(2,1)} fusion(f32[2,32,512]{2,1,0:T(8,128)S(1)} %bitcast_reduce_fusion, f32[32,32]{0,1:T(8,128)S(1)} %fusion.21, f32[2,32]{1,0:T(2,128)S(1)} %fusion.25), kind=kOutput, calls=%fused_computation.5 | convolution fusion | flops 12601344 | bytes 168192 | tf_op jit(solution)/shard_map/gct,gcd->td/dot_general | solution.py:79
  (18 shorter events, 0.1 us)
Async XLA Ops:
  6.5 52.3 %all-gather.2.cloned.1.call-start = ((), (), s32[]{:S(2)}) async-start(), calls=%async_computation.3 | async-start | bytes 1179648 | tf_op jit(solution)/shard_map/all_gather | solution.py:71
  9.1 22.2 %copy-start = (bf16[4,128,4096]{2,1,0:T(8,128)(2,1)S(1)}, bf16[4,128,4096]{2,1,0:T(8,128)(2,1)}, u32[]{:S(2)}) copy-start(bf16[4,128,4096]{2,1,0:T(8,128)(2,1)} %param.17) | copy-start | bytes 12582916
  11.8 21.0 %copy-start.4 = (bf16[4,128,4096]{2,1,0:T(8,128)(2,1)S(1)}, bf16[4,128,4096]{2,1,0:T(8,128)(2,1)}, u32[]{:S(2)}) copy-start(bf16[4,128,4096]{2,1,0:T(8,128)(2,1)} %param.18) | copy-start | bytes 12582916
  32.8 2.3 %copy-start.3 = (s32[8]{0:T(128)S(1)}, s32[8]{0:T(128)}, u32[]{:S(2)}) copy-start(s32[8]{0:T(128)} %param.16) | copy-start | bytes 100
  32.8 2.4 %copy-start.5 = (f32[32]{0:T(128)S(1)}, f32[32]{0:T(128)}, u32[]{:S(2)}) copy-start(f32[32]{0:T(128)} %param.14) | copy-start | bytes 388
  32.8 2.4 %copy-start.1 = (f32[32,4]{0,1:T(4,128)S(1)}, f32[32,4]{0,1:T(4,128)}, u32[]{:S(2)}) copy-start(f32[32,4]{0,1:T(4,128)} %param.15) | copy-start | bytes 1540
  32.8 2.4 %copy-start.2 = (s32[32,4]{0,1:T(4,128)S(1)}, s32[32,4]{0,1:T(4,128)}, u32[]{:S(2)}) copy-start(s32[32,4]{0,1:T(4,128)} %param.13) | copy-start | bytes 1540
Sparse Core Ops, SparseCore 0:
  35.2 23.5 all-gather.1
where the time goes:
time: 81.4 us; the launch traced here: 81.1 us
  blocking collectives  35.2 us (43%)
  waiting for transfers between devices  14.7 us (18%)
  between operations  13.6 us (17%)
  matrix products  12.1 us (15%)
  other arithmetic  4.48 us (6%)
  local copies, waits for them, and re-layouts  1.06 us (1%)
    all_to_all x1, blocking collectives, local(): lax.all_to_all(send_rows, 'ep', split_axis=0, concat_axis=0, tiled=True)  19.4 us
    all_gather x1, waiting for transfers between devices, local(): lax.all_gather(hidden, 'tp', axis=2, tiled=True)  14.7 us
    all_to_all x1, blocking collectives, local(): lax.all_to_all(results, 'ep', split_axis=0, concat_axis=0, tiled=True)  8.79 us
    all_to_all x1, blocking collectives, local(): lax.all_to_all(send_gates, 'ep', split_axis=0, concat_axis=0, tiled=True)  7.01 us
    dot_general x1, matrix products, local(): jnp.einsum('ref,efd->red', lax.all_gather(hidden, 'tp', axis=2, tiled=Tru...  3.23 us
    dot_general x1, matrix products, local(): results = jnp.einsum('re,red->rd', slot_gates, total, precision=highest)  2.43 us
    dot_general x1, matrix products, expert_hidden(): jnp.einsum('rd,efd->ref', rows, w_up, preferred_element_type=jnp.float32)  2.18 us
  transfers between devices with their start and end apart: 1, of which 1 were waited for; matrix products, arithmetic and copies ran while one was open for 2% of the time, Pallas kernels for 0%

commit v1 on v0

--- a/solution.py
+++ b/solution.py
@@ -5,6 +5,22 @@
 
 EXP_PER_GROUP = 8
 STEP_TOK = 4
+
+
+def product_in_turn(shard, axis, dim, term):
+    count, index, rows = (lax.axis_size(axis), lax.axis_index(axis), shard.shape[dim])
+    ahead = [(i, (i + 1) % count) for i in range(count)]
+    backward = [(i, (i - 1) % count) for i in range(count)]
+    middle = count // 2
+    from_left = from_right = shard
+    total = term(shard, index * rows)
+    for turn in range(1, middle + 1):
+        from_left = lax.ppermute(from_left, axis, ahead)
+        if turn < count - middle:
+            from_right = lax.ppermute(from_right, axis, backward)
+            total = total + term(from_right, (index + turn) % count * rows)
+        total = total + term(from_left, (index - turn) % count * rows)
+    return total
 
 
 def norm_rows(tokens, norm_gain):
@@ -66,11 +82,16 @@
     slot_rows = recv_rows.reshape(ep_size * capacity, recv_rows.shape[2])
     slot_gates = recv_gates.reshape(ep_size * capacity, exp_dev)
     hidden = expert_hidden(slot_rows, w_gate, w_up)
-    total = jnp.einsum(
-        "ref,efd->red",
-        lax.all_gather(hidden, "tp", axis=2, tiled=True),
-        w_down,
-        preferred_element_type=jnp.float32,
+    total = product_in_turn(
+        hidden,
+        "tp",
+        2,
+        lambda part, offset: jnp.einsum(
+            "ref,efd->red",
+            part,
+            lax.dynamic_slice_in_dim(w_down, offset, part.shape[2], axis=1),
+            preferred_element_type=jnp.float32,
+        ),
     )
     results = jnp.einsum("re,red->rd", slot_gates, total, precision=highest)
     results = results.reshape(ep_size, capacity, width_part)

time: 81.4 us -> 76.6 us (0.941)
  blocking collectives: 35.2 us -> 8.11 us
  starting transfers between devices: 0.01 us -> 18.2 us
  waiting for transfers between devices: 14.7 us -> 29.2 us
  between operations: 13.6 us -> 0.29 us
  other arithmetic: 4.48 us -> 7 us
  local copies, waits for them, and re-layouts: 1.06 us -> 2.71 us
  matrix products: 12.1 us -> 10.7 us
    all_to_all x2 -> x0, blocking collectives: 26.4 us -> none  [the longest x1 19.4 us: local(): lax.all_to_all(send_rows, 'ep', split_axis=0, concat_axis=0, tiled=True)]
    ppermute x0 -> x7, waiting for transfers between devices: none -> 16.1 us  [the longest x4 16.1 us: product_in_turn(): from_left = lax.ppermute(from_left, axis, ahead)]
    all_gather x1 -> x0, waiting for transfers between devices: 14.7 us -> none  [local(): lax.all_gather(hidden, 'tp', axis=2, tiled=True)]
    all_to_all x0 -> x2, waiting for transfers between devices: none -> 13.1 us  [the longest x1 11 us: local(): lax.all_to_all(send_rows, 'ep', split_axis=0, concat_axis=0, tiled=True)]
    ppermute x0 -> x7, starting transfers between devices: none -> 9.48 us  [the longest x3 9.47 us: product_in_turn(): from_right = lax.ppermute(from_right, axis, backward)]
    all_to_all x0 -> x2, starting transfers between devices: none -> 8.71 us  [the longest x1 5.19 us: local(): lax.all_to_all(send_gates, 'ep', split_axis=0, concat_axis=0, tiled=True)]
    dot_general x2 -> x8, matrix products: 5.65 us -> 2.83 us  [local(): jnp.einsum('ref,efd->red', part, lax.dynamic_slice_in_dim(w_down, offset,...]
    dot_general x1, matrix products: 1.53 us -> 3.86 us  [expert_hidden(): jnp.einsum('rd,efd->ref', rows, w_gate, preferred_element_type=jnp.float32)]
  transfers between devices with their start and end apart: 1 -> 9, of which waited for: 1 -> 6; matrix products, arithmetic and copies ran while one was open for 2% -> 8% of each run, Pallas kernels for 0% -> 0%
where the time goes in v1:
time: 76.6 us; the launch traced here: 76.2 us
  waiting for transfers between devices  29.2 us (38%)
  starting transfers between devices  18.2 us (24%)
  matrix products  10.7 us (14%)
  blocking collectives  8.11 us (11%)
  other arithmetic  7 us (9%)
  local copies, waits for them, and re-layouts  2.71 us (4%)
    ppermute x4, waiting for transfers between devices, product_in_turn(): from_left = lax.ppermute(from_left, axis, ahead)  16.1 us
    all_to_all x1, waiting for transfers between devices, local(): lax.all_to_all(send_rows, 'ep', split_axis=0, concat_axis=0, tiled=True)  11 us
    ppermute x3, starting transfers between devices, product_in_turn(): from_right = lax.ppermute(from_right, axis, backward)  9.47 us
    all_to_all x1, blocking collectives, local(): lax.all_to_all(results, 'ep', split_axis=0, concat_axis=0, tiled=True)  8.11 us
    all_to_all x1, starting transfers between devices, local(): lax.all_to_all(send_gates, 'ep', split_axis=0, concat_axis=0, tiled=True)  5.19 us
    dot_general x1, matrix products, expert_hidden(): jnp.einsum('rd,efd->ref', rows, w_gate, preferred_element_type=jnp.float32)  3.86 us
    all_to_all x1, starting transfers between devices, local(): lax.all_to_all(send_rows, 'ep', split_axis=0, concat_axis=0, tiled=True)  3.51 us
    dot_general x8, matrix products, local(): jnp.einsum('ref,efd->red', part, lax.dynamic_slice_in_dim(w_down, offset,...  2.83 us
  transfers between devices with their start and end apart: 9, of which 6 were waited for; matrix products, arithmetic and copies ran while one was open for 8% of the time, Pallas kernels for 0%

profile of v1, /device:TPU:0, one launch (start us, length us, event | category | flops | bytes accessed | tf_op | source)
XLA Modules:
  0.0 76.2 jit_solution(9749560860275209126)
XLA Ops:
  0.0 0.7 fusion.31
  0.7 0.7 fusion.47
  1.4 0.8 %select_reduce_fusion.1 = s32[32]{0:T(128)S(1)} fusion(s32[32,2]{1,0:T(8,128)S(1)} %reduce_window_sum.11, s32[32]{0:T(128)} %bitcast.52), kind=kLoop, calls=%fused_computation.45 | loop fusion | flops 224 | bytes 512 | tf_op jit(solution)/shard_map/reduce_sum | solution.py:67
  2.4 0.7 fusion.38
  3.1 0.7 broadcast_select_fusion
  3.8 0.7 broadcast_multiply_fusion
  4.4 0.7 select_reduce_fusion
  5.5 0.7 reshape.114
  6.2 5.2 %all-to-all-start = ((f32[4,1,128]{2,1,0:T(1,128)}), f32[4,1,128]{2,1,0:T(1,128)S(1)}, u32[]{:S(2)}, u32[]{:S(2)}) async-start(f32[4,1,128]{2,1,0:T(1,128)} %reshape.114), calls=%async_computation | async-start | bytes 4096 | tf_op jit(solution)/shard_map/all_to_all | solution.py:81
  11.4 1.1 %fusion.7 = f32[32]{0:T(128)S(1)} fusion(bf16[32,4096]{1,0:T(8,128)(2,1)} %param.10), kind=kLoop, calls=%fused_computation.17 | loop fusion | flops 393184 | bytes 262272 | tf_op jit(solution)/shard_map/reduce_sum | solution.py:28
  12.5 1.4 %convolution_convert_fusion = bf16[2,32,4096]{2,1,0:T(8,128)(2,1)S(1)} fusion(bf16[32,4096]{1,0:T(8,128)(2,1)} %param.10, f32[4096]{0:T(1024)} %param.11, f32[32]{0:T(128)S(1)} %add_rsqrt_fusion, f32[32,32]{0,1:T(8,128)S(1)} %fusion.35, f32[2,32]{1,0:T(2,128)S(1)} %fusion.47), kind=kOutput, calls=%fused_computation | convolution fusion | flops 17567744 | bytes 807296 | tf_op jit(solution)/shard_map/gct,td->gcd/dot_general | solution.py:72
  13.9 2.1 %all-to-all-done = f32[4,1,128]{2,1,0:T(1,128)S(1)} async-done(((f32[4,1,128]{2,1,0:T(1,128)}), f32[4,1,128]{2,1,0:T(1,128)S(1)}, u32[]{:S(2)}, u32[]{:S(2)}) %all-to-all-start) | async-done | bytes 2080 | tf_op jit(solution)/shard_map/all_to_all | solution.py:81
  16.0 1.1 %broadcast_in_dim.2 = bf16[2,2,32,4096]{3,2,1,0:T(8,128)(2,1)} broadcast(bf16[2,32,4096]{2,1,0:T(8,128)(2,1)S(1)} %convolution_convert_fusion), dimensions={0,2,3} | broadcast | bytes 1572864 | tf_op jit(solution)/shard_map/broadcast_in_dim | solution.py:77
  17.1 3.5 %all-to-all-start.1 = ((bf16[4,32,4096]{2,1,0:T(8,128)(2,1)}), bf16[4,32,4096]{2,1,0:T(8,128)(2,1)S(1)}, u32[]{:S(2)}, u32[]{:S(2)}) async-start(bf16[4,32,4096]{2,1,0:T(8,128)(2,1)} %bitcast.3), calls=%async_computation.1 | async-start | bytes 2097152 | tf_op jit(solution)/shard_map/all_to_all | solution.py:80
  20.7 0.5 broadcast.128
  21.3 0.7 reduce.2
  22.1 11.0 %all-to-all-done.1 = bf16[4,32,4096]{2,1,0:T(8,128)(2,1)S(1)} async-done(((bf16[4,32,4096]{2,1,0:T(8,128)(2,1)}), bf16[4,32,4096]{2,1,0:T(8,128)(2,1)S(1)}, u32[]{:S(2)}, u32[]{:S(2)}) %all-to-all-start.1) | async-done | bytes 1048608 | tf_op jit(solution)/shard_map/all_to_all | solution.py:80
  33.1 3.9 %fusion.49 = f32[128,4,128]{2,0,1:T(8,128)S(1)} fusion(bf16[128,4096,1]{1,0,2:T(8,128)(2,1)S(1)} %bitcast.45, bf16[4,128,4096]{2,1,0:T(8,128)(2,1)} %param.17), kind=kOutput, calls=%fused_computation.77 | convolution fusion | flops 536870912 | bytes 5505024 | tf_op jit(solution)/shard_map/rd,efd->ref/dot_general | solution.py:42
  37.0 1.5 %fusion.5 = bf16[128,4,128]{2,0,1:T(8,128)(2,1)S(1)} fusion(bf16[128,4096,1]{1,0,2:T(8,128)(2,1)S(1)} %bitcast.46, bf16[4,128,4096]{2,1,0:T(8,128)(2,1)S(1)} %copy-done.1, f32[128,4,128]{2,0,1:T(8,128)S(1)} %fusion.49), kind=kOutput, calls=%fused_computation.12 | convolution fusion | flops 537264128 | bytes 5636096 | tf_op jit(solution)/shard_map/rd,efd->ref/dot_general | solution.py:43
  38.5 2.3 %collective-permute-start = (bf16[128,4,128]{2,0,1:T(8,128)(2,1)S(1)}, bf16[128,4,128]{2,0,1:T(8,128)(2,1)S(1)}, u32[]{:S(2)}, u32[]{:S(2)}) collective-permute-start(bf16[128,4,128]{2,0,1:T(8,128)(2,1)S(1)} %fusion.5), channel_id=1, source_target_pairs={{0,7},{1,0},{2,1},{3,2},{4,3},{5,4},{6,5},{7,6},{8,15},{9,8},{10,9... | collective-permute-start | bytes 393224 | tf_op jit(solution)/shard_map/ppermute | solution.py:20
  41.2 5.8 %collective-permute-done.1 = bf16[128,4,128]{2,0,1:T(8,128)(2,1)S(1)} collective-permute-done((bf16[128,4,128]{2,0,1:T(8,128)(2,1)S(1)}, bf16[128,4,128]{2,0,1:T(8,128)(2,1)S(1)}, u32[]{:S(2)}, u32[]{:S(2)}) %collective-permute-start.1) | collective-permute-done | bytes 131104 | tf_op jit(solution)/shard_map/ppermute | solution.py:18
  47.0 3.5 %collective-permute-start.2 = (bf16[128,4,128]{2,0,1:T(8,128)(2,1)S(1)}, bf16[128,4,128]{2,0,1:T(8,128)(2,1)S(1)}, u32[]{:S(2)}, u32[]{:S(2)}) collective-permute-start(bf16[128,4,128]{2,0,1:T(8,128)(2,1)S(1)} %collective-permute-done), channel_id=1, source_target_pairs={{0,7},{1,0},{2,1},{3,2},{4,3},{5,4},{6,5},{7,6},{8,15},{9,8},{10,9... | collective-permute-start | bytes 393224 | tf_op jit(solution)/shard_map/ppermute | solution.py:20
  50.9 0.4 convolution_add_fusion.3
  51.3 2.9 %collective-permute-done.3 = bf16[128,4,128]{2,0,1:T(8,128)(2,1)S(1)} collective-permute-done((bf16[128,4,128]{2,0,1:T(8,128)(2,1)S(1)}, bf16[128,4,128]{2,0,1:T(8,128)(2,1)S(1)}, u32[]{:S(2)}, u32[]{:S(2)}) %collective-permute-start.3) | collective-permute-done | bytes 131104 | tf_op jit(solution)/shard_map/ppermute | solution.py:18
  54.6 3.6 %collective-permute-start.4 = (bf16[128,4,128]{2,0,1:T(8,128)(2,1)S(1)}, bf16[128,4,128]{2,0,1:T(8,128)(2,1)S(1)}, u32[]{:S(2)}, u32[]{:S(2)}) collective-permute-start(bf16[128,4,128]{2,0,1:T(8,128)(2,1)S(1)} %collective-permute-done.2), channel_id=1, source_target_pairs={{0,7},{1,0},{2,1},{3,2},{4,3},{5,4},{6,5},{7,6},{8,15},{9,8},{10,9... | collective-permute-start | bytes 393224 | tf_op jit(solution)/shard_map/ppermute | solution.py:20
  58.2 0.4 fusion.3
  58.5 1.9 %collective-permute-done.5 = bf16[128,4,128]{2,0,1:T(8,128)(2,1)S(1)} collective-permute-done((bf16[128,4,128]{2,0,1:T(8,128)(2,1)S(1)}, bf16[128,4,128]{2,0,1:T(8,128)(2,1)S(1)}, u32[]{:S(2)}, u32[]{:S(2)}) %collective-permute-start.5) | collective-permute-done | bytes 131104 | tf_op jit(solution)/shard_map/ppermute | solution.py:18
  60.8 0.4 fusion.2
  61.1 5.5 %collective-permute-done.6 = bf16[128,4,128]{2,0,1:T(8,128)(2,1)S(1)} collective-permute-done((bf16[128,4,128]{2,0,1:T(8,128)(2,1)S(1)}, bf16[128,4,128]{2,0,1:T(8,128)(2,1)S(1)}, u32[]{:S(2)}, u32[]{:S(2)}) %collective-permute-start.6) | collective-permute-done | bytes 131104 | tf_op jit(solution)/shard_map/ppermute | solution.py:18
  66.6 0.4 fusion.4
  67.1 8.1 %all_to_all.15 = f32[4,32,512]{2,1,0:T(8,128)S(1)} all-to-all(f32[4,32,512]{2,1,0:T(8,128)S(1)} %bitcast.47), channel_id=1, replica_groups=mesh['ep'=4,'tp'=8] {'ep'}, dimensions={0} | all-to-all | bytes 524288 | tf_op jit(solution)/shard_map/all_to_all | solution.py:98
  75.2 0.9 %fusion.6 = bf16[32,512]{1,0:T(8,128)(2,1)} fusion(f32[2,32,512]{2,1,0:T(8,128)S(1)} %bitcast_reduce_fusion, f32[32,32]{0,1:T(8,128)S(1)} %fusion.35, f32[2,32]{1,0:T(2,128)S(1)} %fusion.47), kind=kOutput, calls=%fused_computation.14 | convolution fusion | flops 12601344 | bytes 168192 | tf_op jit(solution)/shard_map/gct,gcd->td/dot_general | solution.py:100
  (30 shorter events, 2.3 us)
Async XLA Ops:
  6.2 9.8 %all-to-all-start = ((f32[4,1,128]{2,1,0:T(1,128)}), f32[4,1,128]{2,1,0:T(1,128)S(1)}, u32[]{:S(2)}, u32[]{:S(2)}) async-start(f32[4,1,128]{2,1,0:T(1,128)} %reshape.114), calls=%async_computation | async-start | bytes 4096 | tf_op jit(solution)/shard_map/all_to_all | solution.py:81
  17.1 16.0 %all-to-all-start.1 = ((bf16[4,32,4096]{2,1,0:T(8,128)(2,1)}), bf16[4,32,4096]{2,1,0:T(8,128)(2,1)S(1)}, u32[]{:S(2)}, u32[]{:S(2)}) async-start(bf16[4,32,4096]{2,1,0:T(8,128)(2,1)} %bitcast.3), calls=%async_computation.1 | async-start | bytes 2097152 | tf_op jit(solution)/shard_map/all_to_all | solution.py:80
  33.1 3.9 %copy-start.1 = (bf16[4,128,4096]{2,1,0:T(8,128)(2,1)S(1)}, bf16[4,128,4096]{2,1,0:T(8,128)(2,1)}, u32[]{:S(2)}) copy-start(bf16[4,128,4096]{2,1,0:T(8,128)(2,1)} %param.18) | copy-start | bytes 12582916
  36.9 3.9 %copy-start = (bf16[4,1024,512]{2,1,0:T(8,128)(2,1)S(1)}, bf16[4,1024,512]{2,1,0:T(8,128)(2,1)}, u32[]{:S(2)}) copy-start(bf16[4,1024,512]{2,1,0:T(8,128)(2,1)} %param.19) | copy-start | bytes 12582916
  38.5 8.5 %collective-permute-start = (bf16[128,4,128]{2,0,1:T(8,128)(2,1)S(1)}, bf16[128,4,128]{2,0,1:T(8,128)(2,1)S(1)}, u32[]{:S(2)}, u32[]{:S(2)}) collective-permute-start(bf16[128,4,128]{2,0,1:T(8,128)(2,1)S(1)} %fusion.5), channel_id=1, source_target_pairs={{0,7},{1,0},{2,1},{3,2},{4,3},{5,4},{6,5},{7,6},{8,15},{9,8},{10,9... | collective-permute-start | bytes 393224 | tf_op jit(solution)/shard_map/ppermute | solution.py:20
  40.8 6.2 %collective-permute-start.1 = (bf16[128,4,128]{2,0,1:T(8,128)(2,1)S(1)}, bf16[128,4,128]{2,0,1:T(8,128)(2,1)S(1)}, u32[]{:S(2)}, u32[]{:S(2)}) collective-permute-start(bf16[128,4,128]{2,0,1:T(8,128)(2,1)S(1)} %fusion.5), channel_id=1, source_target_pairs={{0,1},{1,2},{2,3},{3,4},{4,5},{5,6},{6,7},{7,0},{8,9},{9,10},{10,1... | collective-permute-start | bytes 393224 | tf_op jit(solution)/shard_map/ppermute | solution.py:18
  47.0 7.2 %collective-permute-start.3 = (bf16[128,4,128]{2,0,1:T(8,128)(2,1)S(1)}, bf16[128,4,128]{2,0,1:T(8,128)(2,1)S(1)}, u32[]{:S(2)}, u32[]{:S(2)}) collective-permute-start(bf16[128,4,128]{2,0,1:T(8,128)(2,1)S(1)} %collective-permute-done.1), channel_id=1, source_target_pairs={{0,1},{1,2},{2,3},{3,4},{4,5},{5,6},{6,7},{7,0},{8,9},{9,10},{10,1... | collective-permute-start | bytes 393224 | tf_op jit(solution)/shard_map/ppermute | solution.py:18
  47.0 7.6 %collective-permute-start.2 = (bf16[128,4,128]{2,0,1:T(8,128)(2,1)S(1)}, bf16[128,4,128]{2,0,1:T(8,128)(2,1)S(1)}, u32[]{:S(2)}, u32[]{:S(2)}) collective-permute-start(bf16[128,4,128]{2,0,1:T(8,128)(2,1)S(1)} %collective-permute-done), channel_id=1, source_target_pairs={{0,7},{1,0},{2,1},{3,2},{4,3},{5,4},{6,5},{7,6},{8,15},{9,8},{10,9... | collective-permute-start | bytes 393224 | tf_op jit(solution)/shard_map/ppermute | solution.py:20
  54.2 6.2 %collective-permute-start.5 = (bf16[128,4,128]{2,0,1:T(8,128)(2,1)S(1)}, bf16[128,4,128]{2,0,1:T(8,128)(2,1)S(1)}, u32[]{:S(2)}, u32[]{:S(2)}) collective-permute-start(bf16[128,4,128]{2,0,1:T(8,128)(2,1)S(1)} %collective-permute-done.3), channel_id=1, source_target_pairs={{0,1},{1,2},{2,3},{3,4},{4,5},{5,6},{6,7},{7,0},{8,9},{9,10},{10,1... | collective-permute-start | bytes 393224 | tf_op jit(solution)/shard_map/ppermute | solution.py:18
  54.6 6.2 %collective-permute-start.4 = (bf16[128,4,128]{2,0,1:T(8,128)(2,1)S(1)}, bf16[128,4,128]{2,0,1:T(8,128)(2,1)S(1)}, u32[]{:S(2)}, u32[]{:S(2)}) collective-permute-start(bf16[128,4,128]{2,0,1:T(8,128)(2,1)S(1)} %collective-permute-done.2), channel_id=1, source_target_pairs={{0,7},{1,0},{2,1},{3,2},{4,3},{5,4},{6,5},{7,6},{8,15},{9,8},{10,9... | collective-permute-start | bytes 393224 | tf_op jit(solution)/shard_map/ppermute | solution.py:20
  60.4 6.2 %collective-permute-start.6 = (bf16[128,4,128]{2,0,1:T(8,128)(2,1)S(1)}, bf16[128,4,128]{2,0,1:T(8,128)(2,1)S(1)}, u32[]{:S(2)}, u32[]{:S(2)}) collective-permute-start(bf16[128,4,128]{2,0,1:T(8,128)(2,1)S(1)} %collective-permute-done.5), channel_id=1, source_target_pairs={{0,1},{1,2},{2,3},{3,4},{4,5},{5,6},{6,7},{7,0},{8,9},{9,10},{10,1... | collective-permute-start | bytes 393224 | tf_op jit(solution)/shard_map/ppermute | solution.py:18
